TPU v7x, 512 devices: a whole 4x4x16 slice. The times are simulated.
512 devices in a mesh: sp: 32 (over z, core), tp: 16 (over y, x).
Axes of the slice: x: 4, y: 4, z: 16, core: 2. Of those that a mesh axis runs over, the one named last changes fastest.
Arguments:
- tokens: bfloat16 [24576, 2048], P('sp', 'tp'), may hold values from -26 to 26, as said below
- mix_gain: bfloat16 [2, 2048], replicated, may hold values from 0.099609375 to 1.8984375
- x_weight: bfloat16 [2, 2048, 1024], P(None, 'sp', 'tp'), may hold values from -0.125 to 0.125
- gate_weight: bfloat16 [2, 2048, 1024], P(None, 'sp', 'tp'), may hold values from -0.125 to 0.125
- conv_taps: bfloat16 [2, 4, 1024], P(None, None, 'tp'), may hold values from -3 to 3
- a_maps: bfloat16 [2, 16, 64, 64], P(None, 'tp'), may hold values from -0.75 to 0.75
- i_maps: bfloat16 [2, 16, 64, 64], P(None, 'tp'), may hold values from -0.75 to 0.75
- decay_rate: float32 [2, 1024], P(None, 'tp'), as said below
- pace: float32 [24576], P('sp'), may hold values from 0.35 to 2.8, as said below
- jumps: float32 [24576], P('sp'), may hold values from -0.7 to 0, as said below
- out_gain: bfloat16 [2, 1024], P(None, 'tp'), may hold values from 0.099609375 to 1.8984375
- out_weight: bfloat16 [2, 1024, 2048], P(None, 'sp', 'tp'), may hold values from -0.1875 to 0.1875
Outputs:
- stream: bfloat16 [24576, 2048], P('sp', 'tp')
Inputs may be any that keep to these rules, and one draw needn't show every extreme that they name: `tokens`: random-looking real values; feature scales differ along the features. `decay_rate`: positive. `pace`: positive. `jumps`: zero or negative.
All inputs are finite; a program needn't handle non-finite values.
Results may differ from a plain program's by a relative error of at most 0.01.
Values may be sent and summed in bfloat16 or wider, within the bound.
A program may use at most 64 MiB of HBM per device.

v0:
```python
import jax
import jax.numpy as jnp
from jax import lax
from jax.sharding import PartitionSpec as P

D_REC = 1024
HEAD = 64
WIDTH = 4
LAYERS = 2


EPS = 1e-06
GATE_C = 8.0


def sent_together(arrays, axis, dim, along):
    ends, at = ([], 0)
    for a in arrays[:-1]:
        at += a.shape[along]
        ends.append(at)
    both = jnp.concatenate(arrays, axis=along)
    return tuple(jnp.split(lax.all_gather(both, axis, axis=dim, tiled=True), ends, axis=along))


def joined_along(parts, dim):
    parts = jnp.moveaxis(parts, 0, dim)
    dims = parts.shape
    return parts.reshape(*dims[:dim], dims[dim] * dims[dim + 1], *dims[dim + 2 :])


def copy_for_each(x, axis):
    copies = jnp.broadcast_to(x, (lax.axis_size(axis), *x.shape))
    return lax.all_to_all(copies, axis, split_axis=0, concat_axis=0, tiled=True)


def gathered_copies(x, axis, dim):
    return joined_along(copy_for_each(x, axis), dim)


def from_behind(x, axis, by):
    peers = lax.axis_size(axis)
    pairs = [(i, i + by) for i in range(peers) if 0 <= i + by < peers]
    return lax.ppermute(x, axis, pairs)


def gathered_once(x, axis):
    leaves = jax.tree.leaves(x)
    turns = sorted(range(len(leaves)), key=lambda k: -leaves[k].size)
    width = (1, *leaves[turns[0]].shape)[-1]
    lines = [
        jnp.pad(leaves[k].reshape(-1), (0, -leaves[k].size % width)).reshape(-1, width)
        for k in turns
    ]
    both, at, found = (copy_for_each(jnp.concatenate(lines), axis), 0, {})
    for k, line in zip(turns, lines):
        share = both[:, at : at + len(line)].reshape(len(both), -1)
        found[k] = share[:, : leaves[k].size].reshape(-1, *leaves[k].shape)
        at += len(line)
    numbers = iter(range(len(leaves)))
    return jax.tree.map(lambda _: found[next(numbers)], x)


def combined_pairwise(pieces, combine):
    while len(jax.tree.leaves(pieces)[0]) > 1:
        pieces = jax.vmap(combine)(
            *(jax.tree.map(lambda part: part[side::2], pieces) for side in (0, 1))
        )
    return jax.tree.map(lambda part: part[0], pieces)


def prefix(x, axis, combine, identity):
    peers, position = (lax.axis_size(axis), lax.axis_index(axis))
    passed = jnp.arange(peers) < position

    def kept(part, zero, own):
        part = jnp.where(
            passed.reshape(-1, *(1 for _ in own.shape)), part, jnp.asarray(zero, own.dtype)
        )
        return part

    pieces = gathered_once(x, axis)
    return combined_pairwise(jax.tree.map(kept, pieces, identity, x), combine)


def taken_together(x, axis):
    everything = copy_for_each(x, axis)
    return jnp.sum(everything, axis=0)


def combine(first, second):
    return (first[0] * second[0], second[0] * first[1] + second[1])


def body(
    tokens,
    mix_gain,
    x_weight,
    gate_weight,
    conv_taps,
    a_maps,
    i_maps,
    decay_rate,
    pace,
    jumps,
    out_gain,
    out_weight,
):
    f32 = jnp.float32
    tok_rows, col_width = tokens.shape
    channels = x_weight.shape[2]
    stream = tokens
    for layer in range(LAYERS):
        w_x, w_gate, w_out = (
            *sent_together((x_weight[layer], gate_weight[layer]), "sp", 0, 1),
            lax.all_gather(out_weight[layer], "sp", axis=0, tiled=True),
        )
        w_both = jnp.concatenate([w_x, w_gate], axis=1)
        xf = stream.astype(f32)
        gain = mix_gain[layer].astype(f32)
        whole = gathered_copies(stream, "tp", 1).astype(f32)
        normed = (
            whole * lax.rsqrt(jnp.mean(whole * whole, axis=1, keepdims=True) + EPS) * gain[None, :]
        ).astype(jnp.bfloat16)
        projected = jnp.einsum("td,dc->ct", normed, w_both, preferred_element_type=f32)
        xr = projected[:channels].astype(jnp.bfloat16)
        gr = projected[channels:].astype(jnp.bfloat16)
        rim = from_behind(xr[:, tok_rows - (WIDTH - 1) :], "sp", 1)
        padded = jnp.concatenate([rim, xr], axis=1).astype(f32)
        taps = conv_taps[layer].astype(f32)
        conv = jnp.zeros((channels, tok_rows), f32)
        for k in range(WIDTH):
            conv = conv + taps[k][:, None] * padded[:, k : k + tok_rows]
        xc = conv.astype(jnp.bfloat16)
        grouped = xc.reshape(channels // HEAD, HEAD, tok_rows)
        rgate = jax.nn.sigmoid(
            jnp.einsum("hij,hit->hjt", a_maps[layer], grouped, preferred_element_type=f32).reshape(
                channels, tok_rows
            )
        )
        igate = jax.nn.sigmoid(
            jnp.einsum("hij,hit->hjt", i_maps[layer], grouped, preferred_element_type=f32).reshape(
                channels, tok_rows
            )
        )
        log_a = -GATE_C * rgate * decay_rate[layer][:, None] * pace[None, :] + jumps[None, :]
        decay = jnp.exp(log_a)
        drive = jnp.sqrt(-jnp.expm1(2.0 * log_a)) * igate * xc.astype(f32)
        decay_run, local_state = lax.associative_scan(combine, (decay, drive), axis=1)
        identity = (jnp.ones((channels,), f32), jnp.zeros((channels,), f32))
        incoming = prefix((decay_run[:, -1], local_state[:, -1]), "sp", combine, identity)
        state = local_state + decay_run * incoming[1][:, None]
        rec = state * jax.nn.gelu(gr.astype(f32))
        mixed = (rec * out_gain[layer].astype(f32)[:, None]).astype(jnp.bfloat16)
        squares = taken_together(jnp.sum(rec * rec, axis=0), "tp")
        out_scale = lax.rsqrt(squares / D_REC + EPS)
        update = jnp.einsum(
            "ct,cd->td", gathered_copies(mixed, "tp", 0), w_out, preferred_element_type=f32
        )
        stream = (xf + update * out_scale[:, None]).astype(jnp.bfloat16)
    return stream


def solution(mesh):
    in_specs = (
        P("sp", "tp"),
        P(),
        P(None, "sp", "tp"),
        P(None, "sp", "tp"),
        P(None, None, "tp"),
        P(None, "tp", None, None),
        P(None, "tp", None, None),
        P(None, "tp"),
        P("sp"),
        P("sp"),
        P(None, "tp"),
        P(None, "sp", "tp"),
    )
    out_specs = P("sp", "tp")
    return jax.shard_map(body, mesh=mesh, in_specs=in_specs, out_specs=out_specs, check_vma=False)
```

profile of v0, /device:TPU:1, one launch (start us, length us, event | category | flops | bytes accessed | tf_op | source)
XLA Modules:
  0.0 426.8 jit_solution(9943520850454563436)
XLA Ops:
  1.1 1.9 broadcast_in_dim.62
  3.0 7.7 %all-to-all-start = ((bf16[16,768,128]{1,2,0:T(8,128)(2,1)}), bf16[16,768,128]{1,2,0:T(8,128)(2,1)S(1)}, u32[]{:S(2)}, u32[]{:S(2)}) async-start(bf16[16,768,128]{1,2,0:T(8,128)(2,1)} %broadcast_in_dim.62), calls=%async_computation | async-start | bytes 6291456 | tf_op jit(solution)/shard_map/all_to_all | solution.py:33
  10.9 41.1 %all_gather.12 = bf16[2048,128]{1,0:T(8,128)(2,1)} all-gather(bf16[64,128]{1,0:T(8,128)(2,1)S(1)} %pad_maximum_fusion.36), channel_id=1, replica_groups=mesh['sp'=32,'tp'=16] {'sp'}, dimensions={0}, use_global_device_ids=true | all-gather | bytes 540672 | tf_op jit(solution)/shard_map/all_gather | solution.py:22
  54.6 10.9 %collective-permute-start = (bf16[64,3]{1,0:T(8,128)(2,1)S(1)}, bf16[64,3]{1,0:T(8,128)(2,1)S(1)}, u32[]{:S(2)}, u32[]{:S(2)}) collective-permute-start(bf16[64,3]{1,0:T(8,128)(2,1)S(1)} %slice.1070), channel_id=1, source_target_pairs={{0,16},{16,32},{32,48},{48,64},{64,80},{80,96},{96,112},{112,128},... | collective-permute-start | bytes 1160 | tf_op jit(solution)/shard_map/ppermute | solution.py:43
  67.1 3.3 slice.832
  70.4 3.3 slice.833
  73.7 3.3 slice.831
  77.0 3.3 slice.835
  80.3 1.9 slice.838
  83.9 1.7 slice.837
  101.1 2.1 slice.895
  103.2 3.3 slice.897
  106.5 3.3 slice.830
  119.8 1.8 pad.252
  127.0 3.3 pad.254
  130.2 3.3 pad.255
  133.6 3.3 pad.236
  136.9 3.5 pad.237
  141.5 17.2 %all-to-all-start.1 = ((f32[32,1,128]{2,1,0:T(1,128)}), f32[32,1,128]{2,1,0:T(1,128)S(1)}, u32[]{:S(2)}, u32[]{:S(2)}) async-start(f32[32,1,128]{2,1,0:T(1,128)} %reshape.196), calls=%async_computation.1 | async-start | bytes 32768 | tf_op jit(solution)/shard_map/all_to_all | solution.py:33
  158.7 11.7 %all-to-all-done.1 = f32[32,1,128]{2,1,0:T(1,128)S(1)} async-done(((f32[32,1,128]{2,1,0:T(1,128)}), f32[32,1,128]{2,1,0:T(1,128)S(1)}, u32[]{:S(2)}, u32[]{:S(2)}) %all-to-all-start.1) | async-done | bytes 16416 | tf_op jit(solution)/shard_map/all_to_all | solution.py:33
  172.9 4.1 all-to-all-start.3
  177.1 6.4 %all-to-all-done.3 = f32[16,1,768]{2,1,0:T(1,128)S(1)} async-done(((f32[16,1,768]{2,1,0:T(1,128)}), f32[16,1,768]{2,1,0:T(1,128)S(1)}, u32[]{:S(2)}, u32[]{:S(2)}) %all-to-all-start.3) | async-done | bytes 49184 | tf_op jit(solution)/shard_map/all_to_all | solution.py:33
  184.8 3.7 all-to-all-start.2
  188.5 30.2 %all-gather = bf16[1,1024,128]{2,1,0:T(8,128)(2,1)S(1)} all-gather(bf16[1,32,128]{2,1,0:T(8,128)(2,1)S(1)} %get-tuple-element.98), channel_id=2, replica_groups=mesh['sp'=32,'tp'=16] {'sp'}, dimensions={1}, use_global_device_ids=true | all-gather | bytes 270336 | tf_op jit(solution)/shard_map/all_gather | solution.py:115
  219.6 1.9 broadcast_in_dim.69
  221.5 6.9 %all-to-all-start.4 = ((bf16[16,768,128]{1,2,0:T(8,128)(2,1)}), bf16[16,768,128]{1,2,0:T(8,128)(2,1)S(1)}, u32[]{:S(2)}, u32[]{:S(2)}) async-start(bf16[16,768,128]{1,2,0:T(8,128)(2,1)} %broadcast_in_dim.69), calls=%async_computation.4 | async-start | bytes 6291456 | tf_op jit(solution)/shard_map/all_to_all | solution.py:33
  228.5 32.5 %all_gather.14 = bf16[2048,128]{1,0:T(8,128)(2,1)} all-gather(bf16[64,128]{1,0:T(8,128)(2,1)S(1)} %pad_maximum_fusion.37), channel_id=1, replica_groups=mesh['sp'=32,'tp'=16] {'sp'}, dimensions={0}, use_global_device_ids=true | all-gather | bytes 540672 | tf_op jit(solution)/shard_map/all_gather | solution.py:22
  261.0 15.4 %all-to-all-done.4 = bf16[16,768,128]{1,2,0:T(8,128)(2,1)S(1)} async-done(((bf16[16,768,128]{1,2,0:T(8,128)(2,1)}), bf16[16,768,128]{1,2,0:T(8,128)(2,1)S(1)}, u32[]{:S(2)}, u32[]{:S(2)}) %all-to-all-start.4) | async-done | bytes 3145760 | tf_op jit(solution)/shard_map/all_to_all | solution.py:33
  278.9 4.7 %collective-permute-start.1 = (bf16[64,3]{1,0:T(8,128)(2,1)S(1)}, bf16[64,3]{1,0:T(8,128)(2,1)S(1)}, u32[]{:S(2)}, u32[]{:S(2)}) collective-permute-start(bf16[64,3]{1,0:T(8,128)(2,1)S(1)} %slice.1137), channel_id=1, source_target_pairs={{0,16},{16,32},{32,48},{48,64},{64,80},{80,96},{96,112},{112,128},... | collective-permute-start | bytes 1160 | tf_op jit(solution)/shard_map/ppermute | solution.py:43
  284.9 3.3 slice.961
  288.2 3.3 slice.962
  291.5 3.3 slice.960
  294.8 3.3 slice.964
  298.2 1.8 slice.967
  301.7 1.7 slice.966
  318.9 1.9 slice.965
  320.8 3.3 slice.1026
  324.1 3.3 slice.959
  337.4 2.1 pad.288
  344.8 3.3 pad.290
  348.1 3.3 pad.291
  351.4 3.3 pad.272
  354.7 3.4 pad.273
  358.7 18.7 %all_to_all.42 = f32[32,1,128]{2,1,0:T(1,128)S(1)} all-to-all(f32[32,1,128]{2,1,0:T(1,128)S(1)} %reshape.198), channel_id=1, replica_groups=mesh['sp'=32,'tp'=16] {'sp'}, dimensions={0} | all-to-all | bytes 32768 | tf_op jit(solution)/shard_map/all_to_all | solution.py:33
  379.3 4.1 all-to-all-start.7
  383.6 6.4 %all-to-all-done.7 = f32[16,1,768]{2,1,0:T(1,128)S(1)} async-done(((f32[16,1,768]{2,1,0:T(1,128)}), f32[16,1,768]{2,1,0:T(1,128)S(1)}, u32[]{:S(2)}, u32[]{:S(2)}) %all-to-all-start.7) | async-done | bytes 49184 | tf_op jit(solution)/shard_map/all_to_all | solution.py:33
  391.3 3.7 all-to-all-start.6
  395.0 30.2 %all-gather.1 = bf16[1,1024,128]{2,1,0:T(8,128)(2,1)S(1)} all-gather(bf16[1,32,128]{2,1,0:T(8,128)(2,1)S(1)} %get-tuple-element.97), channel_id=3, replica_groups=mesh['sp'=32,'tp'=16] {'sp'}, dimensions={1}, use_global_device_ids=true | all-gather | bytes 270336 | tf_op jit(solution)/shard_map/all_gather | solution.py:115
  (405 shorter events, 84.1 us)
Async XLA Ops:
  3.0 7.8 %copy-start.8 = (bf16[2,64,64]{2,1,0:T(8,128)(2,1)S(1)}, bf16[2,64,64]{2,1,0:T(8,128)(2,1)}, u32[]{:S(2)}) copy-start(bf16[2,64,64]{2,1,0:T(8,128)(2,1)} %param.15) | copy-start | bytes 49156
  3.0 7.8 %copy-start.9 = (bf16[2,64,64]{2,1,0:T(8,128)(2,1)S(1)}, bf16[2,64,64]{2,1,0:T(8,128)(2,1)}, u32[]{:S(2)}) copy-start(bf16[2,64,64]{2,1,0:T(8,128)(2,1)} %param.14) | copy-start | bytes 49156
  3.0 7.9 %copy-start.12 = (bf16[2,64]{1,0:T(2,128)(2,1)S(1)}, bf16[2,64]{1,0:T(2,128)(2,1)}, u32[]{:S(2)}) copy-start(bf16[2,64]{1,0:T(2,128)(2,1)} %param.22) | copy-start | bytes 772
  3.0 7.9 %copy-start.13 = (f32[2,64]{1,0:T(2,128)S(1)}, f32[2,64]{1,0:T(2,128)}, u32[]{:S(2)}) copy-start(f32[2,64]{1,0:T(2,128)} %param.19) | copy-start | bytes 1540
  3.0 7.9 %copy-start.11 = (bf16[2,4,64]{2,1,0:T(4,128)(2,1)S(1)}, bf16[2,4,64]{2,1,0:T(4,128)(2,1)}, u32[]{:S(2)}) copy-start(bf16[2,4,64]{2,1,0:T(4,128)(2,1)} %param.16) | copy-start | bytes 3076
  3.0 49.0 %copy-start.7 = (bf16[2,2048]{1,0:T(2,128)(2,1)S(1)}, bf16[2,2048]{1,0:T(2,128)(2,1)}, u32[]{:S(2)}) copy-start(bf16[2,2048]{1,0:T(2,128)(2,1)} %param.13) | copy-start | bytes 24580
  3.0 49.1 %all-to-all-start = ((bf16[16,768,128]{1,2,0:T(8,128)(2,1)}), bf16[16,768,128]{1,2,0:T(8,128)(2,1)S(1)}, u32[]{:S(2)}, u32[]{:S(2)}) async-start(bf16[16,768,128]{1,2,0:T(8,128)(2,1)} %broadcast_in_dim.62), calls=%async_computation | async-start | bytes 6291456 | tf_op jit(solution)/shard_map/all_to_all | solution.py:33
  52.8 1.0 copy-start
  53.8 12.6 %copy-start.14 = (bf16[2,1,64,64]{3,2,1,0:T(8,128)(2,1)S(1)}, bf16[2,1,64,64]{3,2,1,0:T(8,128)(2,1)}, u32[]{:S(2)}) copy-start(bf16[2,1,64,64]{3,2,1,0:T(8,128)(2,1)} %param.17) | copy-start | bytes 49156
  53.8 12.6 %copy-start.16 = (f32[768]{0:T(1024)S(1)}, f32[768]{0:T(1024)}, u32[]{:S(2)}) copy-start(f32[768]{0:T(1024)} %param.21) | copy-start | bytes 9220
  53.8 12.7 %copy-start.17 = (f32[768]{0:T(1024)S(1)}, f32[768]{0:T(1024)}, u32[]{:S(2)}) copy-start(f32[768]{0:T(1024)} %param.20) | copy-start | bytes 9220
  53.8 12.9 %copy-start.15 = (bf16[2,1,64,64]{3,2,1,0:T(8,128)(2,1)S(1)}, bf16[2,1,64,64]{3,2,1,0:T(8,128)(2,1)}, u32[]{:S(2)}) copy-start(bf16[2,1,64,64]{3,2,1,0:T(8,128)(2,1)} %param.18) | copy-start | bytes 49156
  54.6 11.5 %collective-permute-start = (bf16[64,3]{1,0:T(8,128)(2,1)S(1)}, bf16[64,3]{1,0:T(8,128)(2,1)S(1)}, u32[]{:S(2)}, u32[]{:S(2)}) collective-permute-start(bf16[64,3]{1,0:T(8,128)(2,1)S(1)} %slice.1070), channel_id=1, source_target_pairs={{0,16},{16,32},{32,48},{48,64},{64,80},{80,96},{96,112},{112,128},... | collective-permute-start | bytes 1160 | tf_op jit(solution)/shard_map/ppermute | solution.py:43
  67.1 42.7 %copy-start.4 = (f32[64,768]{1,0:T(8,128)}, f32[64,768]{1,0:T(8,128)S(1)}, u32[]{:S(2)}) copy-start(f32[64,768]{1,0:T(8,128)S(1)} %fusion.25) | copy-start | bytes 589828
  73.7 36.1 %copy-start.2 = (f32[64,768]{1,0:T(8,128)}, f32[64,768]{1,0:T(8,128)S(1)}, u32[]{:S(2)}) copy-start(f32[64,768]{1,0:T(8,128)S(1)} %exponential_bitcast_fusion.1) | copy-start | bytes 589828
  112.4 14.4 %slice-start = ((f32[64,768]{1,0:T(8,128)}), f32[64,1]{1,0:T(8,128)S(1)}, s32[]{:S(2)}) async-start(f32[64,768]{1,0:T(8,128)} %copy-done.2), calls=%async_computation.8 | async-start | bytes 65536 | tf_op jit(solution)/shard_map/slice | solution.py:148
  113.3 20.3 %slice-start.2 = ((f32[64,768]{1,0:T(8,128)}), f32[64,1]{1,0:T(8,128)S(1)}, s32[]{:S(2)}) async-start(f32[64,768]{1,0:T(8,128)} %copy-done.4), calls=%async_computation.10 | async-start | bytes 65536 | tf_op jit(solution)/shard_map/slice | solution.py:148
  141.5 29.0 %all-to-all-start.1 = ((f32[32,1,128]{2,1,0:T(1,128)}), f32[32,1,128]{2,1,0:T(1,128)S(1)}, u32[]{:S(2)}, u32[]{:S(2)}) async-start(f32[32,1,128]{2,1,0:T(1,128)} %reshape.196), calls=%async_computation.1 | async-start | bytes 32768 | tf_op jit(solution)/shard_map/all_to_all | solution.py:33
  172.1 16.4 %copy-start.10 = (bf16[2,32,128]{2,1,0:T(8,128)(2,1)S(1)}, bf16[2,32,128]{2,1,0:T(8,128)(2,1)}, u32[]{:S(2)}) copy-start(bf16[2,32,128]{2,1,0:T(8,128)(2,1)} %param.23) | copy-start | bytes 49156
  172.1 46.7 %copy-start.6 = (bf16[768,128]{1,0:T(8,128)(2,1)S(1)}, bf16[768,128]{1,0:T(8,128)(2,1)}, u32[]{:S(2)}) copy-start(bf16[768,128]{1,0:T(8,128)(2,1)} %param.12) | copy-start | bytes 589828
  172.9 10.5 %all-to-all-start.3 = ((f32[16,1,768]{2,1,0:T(1,128)}), f32[16,1,768]{2,1,0:T(1,128)S(1)}, u32[]{:S(2)}, u32[]{:S(2)}) async-start(f32[16,1,768]{2,1,0:T(1,128)} %broadcast_in_dim.68), calls=%async_computation.3 | async-start | bytes 98304 | tf_op jit(solution)/shard_map/all_to_all | solution.py:33
  184.8 34.0 %all-to-all-start.2 = ((bf16[16,64,768]{2,1,0:T(8,128)(2,1)}), bf16[16,64,768]{2,1,0:T(8,128)(2,1)S(1)}, u32[]{:S(2)}, u32[]{:S(2)}) async-start(bf16[16,64,768]{2,1,0:T(8,128)(2,1)} %broadcast_in_dim.67), calls=%async_computation.2 | async-start | bytes 3145728 | tf_op jit(solution)/shard_map/all_to_all | solution.py:33
  221.5 54.9 %all-to-all-start.4 = ((bf16[16,768,128]{1,2,0:T(8,128)(2,1)}), bf16[16,768,128]{1,2,0:T(8,128)(2,1)S(1)}, u32[]{:S(2)}, u32[]{:S(2)}) async-start(bf16[16,768,128]{1,2,0:T(8,128)(2,1)} %broadcast_in_dim.69), calls=%async_computation.4 | async-start | bytes 6291456 | tf_op jit(solution)/shard_map/all_to_all | solution.py:33
  277.1 1.0 copy-start.1
  278.9 5.1 %collective-permute-start.1 = (bf16[64,3]{1,0:T(8,128)(2,1)S(1)}, bf16[64,3]{1,0:T(8,128)(2,1)S(1)}, u32[]{:S(2)}, u32[]{:S(2)}) collective-permute-start(bf16[64,3]{1,0:T(8,128)(2,1)S(1)} %slice.1137), channel_id=1, source_target_pairs={{0,16},{16,32},{32,48},{48,64},{64,80},{80,96},{96,112},{112,128},... | collective-permute-start | bytes 1160 | tf_op jit(solution)/shard_map/ppermute | solution.py:43
  284.9 42.5 %copy-start.5 = (f32[64,768]{1,0:T(8,128)}, f32[64,768]{1,0:T(8,128)S(1)}, u32[]{:S(2)}) copy-start(f32[64,768]{1,0:T(8,128)S(1)} %fusion.13) | copy-start | bytes 589828
  291.5 35.9 %copy-start.3 = (f32[64,768]{1,0:T(8,128)}, f32[64,768]{1,0:T(8,128)S(1)}, u32[]{:S(2)}) copy-start(f32[64,768]{1,0:T(8,128)S(1)} %exponential_bitcast_fusion) | copy-start | bytes 589828
  330.0 14.7 %slice-start.1 = ((f32[64,768]{1,0:T(8,128)}), f32[64,1]{1,0:T(8,128)S(1)}, s32[]{:S(2)}) async-start(f32[64,768]{1,0:T(8,128)} %copy-done.3), calls=%async_computation.9 | async-start | bytes 65536 | tf_op jit(solution)/shard_map/slice | solution.py:148
  330.8 20.5 %slice-start.3 = ((f32[64,768]{1,0:T(8,128)}), f32[64,1]{1,0:T(8,128)S(1)}, s32[]{:S(2)}) async-start(f32[64,768]{1,0:T(8,128)} %copy-done.5), calls=%async_computation.11 | async-start | bytes 65536 | tf_op jit(solution)/shard_map/slice | solution.py:148
  379.3 10.6 %all-to-all-start.7 = ((f32[16,1,768]{2,1,0:T(1,128)}), f32[16,1,768]{2,1,0:T(1,128)S(1)}, u32[]{:S(2)}, u32[]{:S(2)}) async-start(f32[16,1,768]{2,1,0:T(1,128)} %broadcast_in_dim.72), calls=%async_computation.7 | async-start | bytes 98304 | tf_op jit(solution)/shard_map/all_to_all | solution.py:33
  391.3 34.0 %all-to-all-start.6 = ((bf16[16,64,768]{2,1,0:T(8,128)(2,1)}), bf16[16,64,768]{2,1,0:T(8,128)(2,1)S(1)}, u32[]{:S(2)}, u32[]{:S(2)}) async-start(bf16[16,64,768]{2,1,0:T(8,128)(2,1)} %broadcast_in_dim.71), calls=%async_computation.6 | async-start | bytes 3145728 | tf_op jit(solution)/shard_map/all_to_all | solution.py:33
where the time goes:
time: 431 us; the launch traced here: 427 us
  local copies, waits for them, and re-layouts  153 us (35%)
  blocking collectives  153 us (35%)
  starting transfers between devices  63 us (15%)
  waiting for transfers between devices  40.9 us (9%)
  other arithmetic  10.9 us (3%)
    slice x112, local copies, waits for them, and re-layouts, body(): lax.associative_scan(combine, (decay, drive), axis=1)  84.2 us
    all_gather x2, blocking collectives, sent_together(): lax.all_gather(both, axis, axis=dim, tiled=True)  73.7 us
    all_gather x2, blocking collectives, body(): lax.all_gather(out_weight[layer], 'sp', axis=0, tiled=True)  60.4 us
    pad x68, local copies, waits for them, and re-layouts, body(): lax.associative_scan(combine, (decay, drive), axis=1)  56.4 us
    all_to_all x7, starting transfers between devices, copy_for_each(): return lax.all_to_all(copies, axis, split_axis=0, concat_axis=0, tiled=True)  47.4 us
    all_to_all x7, waiting for transfers between devices, copy_for_each(): return lax.all_to_all(copies, axis, split_axis=0, concat_axis=0, tiled=True)  39.9 us
    all_to_all x1, blocking collectives, copy_for_each(): return lax.all_to_all(copies, axis, split_axis=0, concat_axis=0, tiled=True)  18.7 us
    ppermute x2, starting transfers between devices, from_behind(): return lax.ppermute(x, axis, pairs)  15.5 us
  transfers between devices with their start and end apart: 9, of which 6 were waited for; matrix products, arithmetic and copies ran while one was open for 0% of the time, Pallas kernels for 0%

commit v1 on v0

v1 whole, which is shorter than its diff:
```python
import functools

import jax
import jax.numpy as jnp
from jax import lax
from jax.experimental import pallas as pl
from jax.experimental.pallas import tpu as pltpu
from jax.sharding import PartitionSpec as P

HEAD = 64
WIDTH = 4
LAYERS = 2
EPS = 1e-06
GATE_C = 8.0
RIM = 16
LANE = 128
ROWS = 8

f32 = jnp.float32
bf16 = jnp.bfloat16


def swapped(x):
    return pltpu.roll(x, HEAD, 1)


def lower_half(shape):
    return lax.broadcasted_iota(jnp.int32, shape, len(shape) - 1) < HEAD


def halves(first, second):
    return jnp.where(lower_half(first.shape), first, second)


def chained(first, second):
    low = lower_half(second.shape)
    return jnp.where(low, second, swapped(second)) * first + jnp.where(low, 0.0, second)


def gelu(x):
    return 0.5 * x * (1.0 + jnp.tanh(0.7978845608028654 * (x + 0.044715 * (x * x * x))))


def one_minus_exp(y, decay):
    series = jnp.ones_like(y)
    for k in range(8, 1, -1):
        series = 1.0 - (y * (1.0 / k)) * series
    return jnp.where(y < 0.5, y * series, 1.0 - decay * decay)


def kernel(n, tq, tok, gain, wxg, wo, maps, small, pj, out,
           WX, WO, MAPS, SMALL, XM, XH, NRM, XR, GEL, BD, PAR, AS, BS, LOC, ACU, MIX, MX,
           PO, PR, ZO, ZR, FS, OB, send, recv):
    nt, nz, ns = n * n, n * n, 2 * n * n
    C = n * HEAD
    pairs = n // 2
    D = nt * LANE
    steps = tq // ROWS
    s, tp = lax.axis_index("sp"), lax.axis_index("tp")
    c, z = s % 2, s // 2
    a, b = z // n, z % n
    y, x = tp // n, tp % n
    p, q = x + c * (y - x), y + c * (x - y)

    def tp_of(core, pp, qq):
        return (qq * n + pp) + core * ((pp * n + qq) - (qq * n + pp))

    sent = []
    numbers = iter(range(10000))

    def put(src, dst, sp_to, tp_to, slot=None):
        slot = next(numbers) if slot is None else slot
        cp = pltpu.make_async_remote_copy(
            src_ref=src, dst_ref=dst, send_sem=send, recv_sem=recv.at[slot],
            device_id={"sp": sp_to, "tp": tp_to}, device_id_type=pl.DeviceIdType.MESH)
        cp.start()
        sent.append(cp)
        return cp

    def landed(copies):
        for cp in copies:
            cp.wait_recv()

    def landed_all(ref, slot):
        pltpu.make_async_copy(ref, ref, recv.at[slot]).wait()

    near = range(1, n)

    def z1_x(l):
        return [put(wxg.at[l], WX.at[l, p, a, b, c], (((a + d) % n) * n + b) * 2 + c, tp) for d in near]

    i0, i1 = a + c * (b - a), b + c * (a - b)

    def z1_o(l):
        return [put(wo.at[l], WO.at[l, p, i0, i1, c], (((a + d) % n) * n + b) * 2 + c, tp) for d in near]

    def z2_x(l):
        ref = WX.at[l, p, :, b, c]
        return [put(ref, ref, (a * n + (b + d) % n) * 2 + c, tp) for d in near]

    def z2_o(l):
        made = []
        for d in near:
            for k in range(n):
                ref = WO.at[l, p, k + c * (b - k), b + c * (k - b), c]
                made.append(put(ref, ref, (a * n + (b + d) % n) * 2 + c, tp))
        return made

    def twin_x(l):
        return [put(WX.at[l, p, :, :, c], WX.at[l, q, :, :, c], z * 2 + 1 - c, tp)]

    def twin_o(l):
        return [put(WO.at[l, p, k, :, c], WO.at[l, q, :, k, c], z * 2 + 1 - c, tp) for k in range(n)]

    def across(ref):
        return [put(ref, ref, s, tp_of(c, (p + d) % n, q)) for d in near]

    own = pl.ds(pl.multiple_of(p * tq, tq), tq)
    t_a = []
    for d in near:
        pp = (p + d) % n
        rows = pl.ds(pl.multiple_of(pp * tq, tq), tq)
        t_a.append(put(tok.at[rows], XM.at[0, tp], s, tp_of(c, pp, q)))
    rim0 = next(numbers)
    rim_sends = []
    for k in range(n):
        e, pp = (k + 1) // n, (k + 1) % n
        src = tok.at[(k + 1) * tq - RIM:(k + 1) * tq]
        for qq in range(n):
            cp = pltpu.make_async_remote_copy(
                src_ref=src, dst_ref=XH.at[0, tp], send_sem=send, recv_sem=recv.at[rim0],
                device_id={"sp": (s + e) % ns, "tp": tp_of((c + e) % 2, pp, qq)},
                device_id_type=pl.DeviceIdType.MESH)
            if e:
                cp.start()
                sent.append(cp)
            else:
                mine = (1 - jnp.minimum(abs(pp - p), 1)) * (1 - jnp.minimum(abs(qq - q), 1))

                @pl.when(mine == 0)
                def _():
                    cp.start()

                @pl.when(mine == 1)
                def _():
                    XH[0, tp] = src[...]
                rim_sends.append((cp, mine))
    wx = [z1_x(0), None]
    wout = [z1_o(0), None]
    m_in = [put(maps, MAPS.at[p], s, tp_of(c, (p + d) % n, q)) for d in near]
    s_in = [put(small, SMALL.at[tp], s, (tp + d) % nt) for d in range(1, nt)]
    wx[1], wout[1] = z1_x(1), z1_o(1)

    XM[0, tp] = tok[own]
    for l in range(LAYERS):
        WX[l, p, a, b, c] = wxg[l]
        WO[l, p, i0, i1, c] = wo[l]
    MAPS[p] = maps[...]
    SMALL[tp] = small[...]

    landed(t_a)
    t_b = []
    for d in near:
        to = tp_of(c, p, (q + d) % n)
        t_b.append(put(tok.at[own], XM.at[0, tp], s, to))
        for e in near:
            ref = XM.at[0, tp_of(c, (p + e) % n, q)]
            t_b.append(put(ref, ref, s, to))

    landed(wx[0])
    wx[0] = z2_x(0)
    landed(wout[0])
    wout[0] = z2_o(0)

    landed(m_in)
    landed(s_in)
    for l in range(LAYERS):
        for jp in range(pairs):
            even = MAPS[2 * jp, l].astype(f32)
            odd = MAPS[2 * jp + 1, l].astype(f32)
            low = lower_half(even.shape)
            BD[l, jp, :HEAD, :LANE] = jnp.where(low, even, 0.0).astype(bf16)
            BD[l, jp, :HEAD, LANE:] = jnp.where(low, swapped(even), 0.0).astype(bf16)
            BD[l, jp, HEAD:, :LANE] = jnp.where(low, 0.0, swapped(odd)).astype(bf16)
            BD[l, jp, HEAD:, LANE:] = jnp.where(low, 0.0, odd).astype(bf16)
            for qq in range(n):
                PAR[l, qq, jp] = halves(SMALL[tp_of(c, 2 * jp, qq), l], SMALL[tp_of(c, 2 * jp + 1, qq), l])

    def norm_rows(l, block, row):
        total = jnp.zeros((RIM, LANE), f32)
        for t in range(nt):
            v = block(t).astype(f32)
            total = total + v * v
        r = lax.rsqrt(jnp.sum(total, axis=1, keepdims=True) * (1.0 / D) + EPS)
        for t in range(nt):
            cols = slice(t * LANE, (t + 1) * LANE)
            g = gain[l:l + 1, cols].astype(f32)
            NRM[pl.ds(row, RIM), cols] = (block(t).astype(f32) * r * g).astype(bf16)

    def norm(l):
        norm_rows(l, lambda t: XH[l, t], 0)

        @pl.loop(0, tq // RIM)
        def _(i):
            row = pl.multiple_of(i * RIM, RIM)
            norm_rows(l, lambda t: XM[l, t, pl.ds(row, RIM), :], pl.multiple_of(row + RIM, RIM))

    def first_half(l):
        keep = jnp.minimum(s + p, 1).astype(f32)
        normed = NRM[...]
        pace = pj[own, 0:1]
        jump = pj[own, 1:2]
        for jp in range(pairs):
            w = jnp.concatenate(
                [WX[l, 2 * jp].reshape(D, LANE), WX[l, 2 * jp + 1].reshape(D, LANE)], axis=1)
            pr = jnp.dot(normed, w, preferred_element_type=f32).astype(bf16).astype(f32)
            left, right = pr[:, :LANE], pr[:, LANE:]
            xr = halves(left, swapped(right))
            XR[jp, :RIM] = xr[:RIM] * keep
            XR[jp, RIM:] = xr[RIM:]
            GEL[jp] = gelu(halves(swapped(left), right)[RIM:])
            par = PAR[l, q, jp]
            conv = jnp.zeros((tq, LANE), f32)
            for k in range(WIDTH):
                conv = conv + par[k:k + 1] * XR[jp, pl.ds(RIM - WIDTH + 1 + k, tq), :]
            xc = conv.astype(bf16)
            gates = jnp.dot(xc, BD[l, jp], preferred_element_type=f32)
            r = jax.nn.sigmoid(gates[:, :LANE])
            gin = jax.nn.sigmoid(gates[:, LANE:])
            log_a = -GATE_C * r * par[4:5] * pace + jump
            decay = jnp.exp(log_a)
            AS[jp] = decay
            BS[jp] = jnp.sqrt(one_minus_exp(-2.0 * log_a, decay)) * gin * xc.astype(f32)
        starts = []
        for jp in range(pairs):
            run = h = None
            for k in range(steps):
                ak = AS[jp, pl.ds(k, ROWS, stride=steps), :]
                bk = BS[jp, pl.ds(k, ROWS, stride=steps), :]
                h = bk if k == 0 else ak * h + bk
                run = ak if k == 0 else ak * run
                LOC[jp, k], ACU[jp, k] = h, run
            row = lax.broadcasted_iota(jnp.int32, (ROWS, LANE), 0)
            for d in (1, 2, 4):
                before = row >= d
                h = run * jnp.where(before, pltpu.roll(h, d, 0), 0.0) + h
                run = run * jnp.where(before, pltpu.roll(run, d, 0), 1.0)
            av, sv = run[ROWS - 1:], h[ROWS - 1:]
            PO[l, 2 * jp] = halves(av, swapped(sv))
            PO[l, 2 * jp + 1] = halves(swapped(av), sv)
            starts.append((jnp.where(row >= 1, pltpu.roll(run, 1, 0), 1.0),
                           jnp.where(row >= 1, pltpu.roll(h, 1, 0), 0.0)))
        return starts

    def prefix(l):
        made = []
        for d in near:
            made.append(put(PO.at[l], PR.at[l, c, p], s, tp_of(c, (p + d) % n, q)))
        slot = next(numbers)
        for k in range(n):
            for pp in range(n):
                put(PO.at[l, k], PR.at[l, c, p, q], z * 2 + 1 - c, tp_of(1 - c, pp, k), slot)
        for j in range(n):
            PR[l, c, p, j] = PO[l, j]
        landed(made)
        landed_all(PR.at[l, 1 - c], slot)
        identity = jnp.where(lower_half((n, LANE)), 1.0, 0.0)
        total = within = identity
        mine = c * n + p
        for i in range(2 * n):
            piece = jnp.concatenate([PR[l, i // n, i % n, j] for j in range(n)], axis=0)
            within = jnp.where(i < mine, chained(within, piece), within)
            total = chained(total, piece)
        for j in range(n):
            ZO[l, j] = total[j:j + 1]
        slot = next(numbers)
        for d in range(1, nz):
            put(ZO.at[l], ZR.at[l, d - 1], ((z + d) % nz) * 2 + c, tp, slot)
        landed_all(ZR.at[l], slot)
        before = identity
        for d in range(nz - 1, 0, -1):
            piece = jnp.concatenate([ZR[l, d - 1, j] for j in range(n)], axis=0)
            before = jnp.where(d <= z, chained(before, piece), before)
        return chained(before, within)

    def second_half(l, starts, incoming):
        turned = swapped(incoming)
        for jp in range(pairs):
            start_run, start_h = starts[jp]
            carry = start_h + start_run * halves(turned[2 * jp:2 * jp + 1], incoming[2 * jp + 1:2 * jp + 2])
            out_gain = PAR[l, q, jp][5:6]
            for k in range(steps):
                rows = pl.ds(k, ROWS, stride=steps)
                MIX[jp, rows, :] = (LOC[jp, k] + ACU[jp, k] * carry) * GEL[jp, rows, :] * out_gain
            MX[l, q, :, jp * LANE:(jp + 1) * LANE] = MIX[jp].astype(bf16)
        return [put(MX.at[l, q], MX.at[l, q], s, tp_of(c, p, (q + d) % n)) for d in near]

    def update(l, emit):
        squares = jnp.zeros((tq, LANE), f32)
        for qq in range(n):
            for jp in range(pairs):
                v = MX[l, qq, :, jp * LANE:(jp + 1) * LANE].astype(f32) / PAR[l, qq, jp][5:6]
                squares = squares + v * v
        scale = lax.rsqrt(jnp.sum(squares, axis=1, keepdims=True) * (1.0 / (n * C)) + EPS)
        mixed = jnp.concatenate([MX[l, qq] for qq in range(n)], axis=1)
        for jp in range(pairs):
            w = jnp.concatenate(
                [WO[l, 2 * jp].reshape(n * C, LANE), WO[l, 2 * jp + 1].reshape(n * C, LANE)], axis=1)
            up = jnp.dot(mixed, w, preferred_element_type=f32) * scale
            for j in (0, 1):
                at = tp_of(c, 2 * jp + j, q)
                emit(2 * jp + j, (XM[l, at].astype(f32) + up[:, j * LANE:(j + 1) * LANE]).astype(bf16))

    landed(t_b)

    @pl.when(p > 0)
    def _():
        landed_all(XH.at[0, :nt - 1], rim0)

    @pl.when(p == 0)
    def _():
        landed_all(XH.at[0], rim0)

    norm(0)
    landed(wx[0])
    wx[0] = twin_x(0)
    landed(wout[0])
    wout[0] = twin_o(0)
    landed(wx[0])
    wx[0] = across(WX.at[0, p])
    landed(wout[0])
    wout[0] = across(WO.at[0, p])
    landed(wx[1])
    wx[1] = z2_x(1)
    landed(wout[1])
    wout[1] = z2_o(1)
    landed(wx[0])
    start = first_half(0)
    landed(wx[1])
    wx[1] = twin_x(1)
    landed(wout[1])
    wout[1] = twin_o(1)
    incoming = prefix(0)
    gathered = second_half(0, start, incoming)
    landed(wx[1])
    wx[1] = across(WX.at[1, p])
    landed(wout[1])
    wout[1] = across(WO.at[1, p])
    landed(wout[0])
    landed(gathered)

    def keep_stream(j, v):
        XM[1, tp_of(c, j, q)] = v

    update(0, keep_stream)
    gathered = []
    for d in near:
        for j in range(n):
            ref = XM.at[1, tp_of(c, j, q)]
            gathered.append(put(ref, ref, s, tp_of(c, p, (q + d) % n)))
    rim1 = next(numbers)
    e, pp = (p + 1) // n, (p + 1) % n
    for j in range(n):
        at = tp_of(c, j, q)
        for qq in range(n):
            put(XM.at[1, at, tq - RIM:tq], XH.at[1, at], (s + e) % ns, tp_of((c + e) % 2, pp, qq), rim1)
    landed(gathered)
    landed_all(XH.at[1], rim1)
    norm(1)
    landed(wx[1])
    start = first_half(1)
    incoming = prefix(1)
    gathered = second_half(1, start, incoming)
    landed(wout[1])
    landed(gathered)

    def keep_last(j, v):
        FS[j] = v

    update(1, keep_last)
    last = [put(FS.at[(p + d) % n], OB.at[p], s, tp_of(c, (p + d) % n, q)) for d in near]
    OB[p] = FS[p]
    landed(last)
    for k in range(n):
        out[k * tq:(k + 1) * tq] = OB[k]
    for cp in sent:
        cp.wait_send()
    for cp, mine in rim_sends:
        @pl.when(mine == 0)
        def _():
            cp.wait_send()


def body(tokens, mix_gain, x_weight, gate_weight, conv_taps, a_maps, i_maps, decay_rate, pace, jumps,
         out_gain, out_weight):
    nt = lax.axis_size("tp")
    n = int(round(nt ** 0.5))
    tq = tokens.shape[0] // n
    C = n * HEAD
    D = nt * LANE
    wxg = jnp.concatenate([x_weight, gate_weight], axis=2)
    maps = jnp.concatenate([a_maps[:, 0], i_maps[:, 0]], axis=2)
    small = jnp.concatenate(
        [conv_taps.astype(f32), decay_rate[:, None], out_gain.astype(f32)[:, None],
         jnp.ones((LAYERS, 2, HEAD), f32)], axis=1)
    small = jnp.concatenate([small, small], axis=2)
    pj = jnp.stack([pace, jumps], axis=1)
    vmem = pl.BlockSpec(memory_space=pltpu.VMEM)
    xr, orr = wxg.shape[1], out_weight.shape[1]
    scratch = [
        pltpu.VMEM((LAYERS, n, n, n, 2, xr, LANE), bf16),
        pltpu.VMEM((LAYERS, n, n, n, 2, orr, LANE), bf16),
        pltpu.VMEM((n, LAYERS, HEAD, LANE), bf16),
        pltpu.VMEM((nt, LAYERS, ROWS, LANE), f32),
        pltpu.VMEM((LAYERS, nt, tq, LANE), bf16),
        pltpu.VMEM((LAYERS, nt, RIM, LANE), bf16),
        pltpu.VMEM((RIM + tq, D), bf16),
        pltpu.VMEM((n // 2, RIM + tq, LANE), f32),
        pltpu.VMEM((n // 2, tq, LANE), f32),
        pltpu.VMEM((LAYERS, n // 2, LANE, 2 * LANE), bf16),
        pltpu.VMEM((LAYERS, n, n // 2, ROWS, LANE), f32),
        pltpu.VMEM((n // 2, tq, LANE), f32),
        pltpu.VMEM((n // 2, tq, LANE), f32),
        pltpu.VMEM((n // 2, tq // ROWS, ROWS, LANE), f32),
        pltpu.VMEM((n // 2, tq // ROWS, ROWS, LANE), f32),
        pltpu.VMEM((n // 2, tq, LANE), f32),
        pltpu.VMEM((LAYERS, n, tq, C), bf16),
        pltpu.VMEM((LAYERS, n, 1, LANE), f32),
        pltpu.VMEM((LAYERS, 2, n, n, 1, LANE), f32),
        pltpu.VMEM((LAYERS, n, 1, LANE), f32),
        pltpu.VMEM((LAYERS, nt - 1, n, 1, LANE), f32),
        pltpu.VMEM((n, tq, LANE), bf16),
        pltpu.VMEM((n, tq, LANE), bf16),
        pltpu.SemaphoreType.DMA,
        pltpu.SemaphoreType.DMA((256,)),
    ]
    return pl.pallas_call(
        functools.partial(kernel, n, tq),
        out_shape=jax.ShapeDtypeStruct(tokens.shape, bf16),
        in_specs=[vmem] * 7,
        out_specs=vmem,
        scratch_shapes=scratch,
        compiler_params=pltpu.CompilerParams(has_side_effects=True, vmem_limit_bytes=56 * 1024 * 1024),
    )(tokens, mix_gain, wxg, out_weight, maps, small, pj)


def solution(mesh):
    in_specs = (
        P("sp", "tp"),
        P(),
        P(None, "sp", "tp"),
        P(None, "sp", "tp"),
        P(None, None, "tp"),
        P(None, "tp", None, None),
        P(None, "tp", None, None),
        P(None, "tp"),
        P("sp"),
        P("sp"),
        P(None, "tp"),
        P(None, "sp", "tp"),
    )
    return jax.shard_map(body, mesh=mesh, in_specs=in_specs, out_specs=P("sp", "tp"), check_vma=False)
```

time: 431 us -> 141 us (0.33)
  blocking collectives: 153 us -> 0 us
  local copies, waits for them, and re-layouts: 153 us -> 5.29 us
  Pallas kernels: 0 us -> 133 us
  starting transfers between devices: 63 us -> 0 us
  waiting for transfers between devices: 40.9 us -> 0 us
  other arithmetic: 10.9 us -> 2.85 us
    all_gather x4 -> x0, blocking collectives: 134 us -> none  [the longest x2 73.7 us: sent_together(): lax.all_gather(both, axis, axis=dim, tiled=True)]
    pallas_call x0 -> x1, Pallas kernels: none -> 133 us  [body(): pl.pallas_call(functools.partial(kernel, n, tq), out_shape=jax.ShapeDtype...]
    slice x151 -> x0, local copies, waits for them, and re-layouts: 85 us -> none  [the longest x112 84.2 us: body(): lax.associative_scan(combine, (decay, drive), axis=1)]
    pad x68 -> x0, local copies, waits for them, and re-layouts: 56.4 us -> none  [body(): lax.associative_scan(combine, (decay, drive), axis=1)]
    all_to_all x7 -> x0, starting transfers between devices: 47.4 us -> none  [copy_for_each(): return lax.all_to_all(copies, axis, split_axis=0, concat_axis=0, tiled=True)]
    all_to_all x7 -> x0, waiting for transfers between devices: 39.9 us -> none  [copy_for_each(): return lax.all_to_all(copies, axis, split_axis=0, concat_axis=0, tiled=True)]
    all_to_all x1 -> x0, blocking collectives: 18.7 us -> none  [copy_for_each(): return lax.all_to_all(copies, axis, split_axis=0, concat_axis=0, tiled=True)]
    ppermute x2 -> x0, starting transfers between devices: 15.5 us -> none  [from_behind(): return lax.ppermute(x, axis, pairs)]
  transfers between devices with their start and end apart: 9 -> 0, of which waited for: 6 -> 0; matrix products, arithmetic and copies ran while one was open for 0% -> 0% of each run, Pallas kernels for 0% -> 0%
where the time goes in v1:
time: 141 us
  Pallas kernels  133 us (94%)
  local copies, waits for them, and re-layouts  5.29 us (4%)
  other arithmetic  2.85 us (2%)
    pallas_call x1, Pallas kernels, body(): pl.pallas_call(functools.partial(kernel, n, tq), out_shape=jax.ShapeDtype...  133 us
    unnamed x7, local copies, waits for them, and re-layouts  2.97 us

profile of v1, /device:TPU:1, one launch (start us, length us, event | category | flops | bytes accessed | tf_op | source)
XLA Modules:
  0.0 140.8 jit_solution(3890879264355365770)
XLA Ops:
  0.0 0.0 copy-start
  0.0 0.7 bitcast_convert_fusion
  0.7 0.7 stack.9
  1.4 0.7 stack.10
  2.0 0.0 copy-start.1
  2.1 0.7 copy-done.1
  2.7 0.0 copy-start.2
  2.7 0.7 copy-done.2
  3.4 0.7 maximum_maximum_fusion.small
  4.1 0.0 copy-done
  4.1 1.5 %pad_maximum_fusion = (bf16[2,64,128]{2,1,0:T(8,128)(2,1)}, bf16[2,64,128]{2,1,0:T(8,128)(2,1)}) fusion(bf16[2,64,64]{2,1,0:T(8,128)(2,1)S(1)} %copy-done, bf16[2,64,64]{2,1,0:T(8,128)(2,1)} %param.14, bf16[2,64,64]{2,1,0:T(8,128)(2,1)} %bitcast.9, bf16[2,64,64]{2,1,0:T(8,128)(2,1)} %bitcast.10), kind=kLoop, calls=%fused_computation | loop fusion | flops 131072 | bytes 131072 | tf_op jit(solution)/shard_map/concatenate | solution.py:401
  5.6 0.9 copy.21.pj
  6.5 132.7 %shard_map.118 = bf16[768,128]{1,0:T(8,128)(2,1)} custom-call(bf16[768,128]{1,0:T(8,128)(2,1)} %tok.1, bf16[2,2048]{1,0:T(2,128)(2,1)} %gain.1, bf16[2,64,128]{2,1,0:T(8,128)(2,1)} %get-tuple-element.5.wxg, bf16[2,32,128]{2,1,0:T(8,128)(2,1)} %wo.1, bf16[2,64,128]{2,1,0:T(8,128)(2,1)} %get-tuple-element.6.maps, f32[2,8,128]{2,1,0:T(8,128)} %maximum_maximum_fusion.small, ...), custom_call_target="tpu_custom_call" | custom-call | tf_op jit(solution)/shard_map/pallas_call | solution.py:437
  139.2 1.6 %copy.23 = bf16[768,128]{1,0:T(8,128)(2,1)} copy(bf16[768,128]{1,0:T(8,128)(2,1)} %shard_map.118) | data formatting | bytes 393216
  (3 shorter events, 0.0 us)
Async XLA Ops:
  0.0 4.1 %copy-start = (bf16[2,64,64]{2,1,0:T(8,128)(2,1)S(1)}, bf16[2,64,64]{2,1,0:T(8,128)(2,1)}, u32[]{:S(2)}) copy-start(bf16[2,64,64]{2,1,0:T(8,128)(2,1)} %param.15) | copy-start | bytes 49156
  2.0 0.7 copy-start.1
  2.7 0.7 copy-start.2

commit v2 on v1

--- a/solution.py
+++ b/solution.py
@@ -48,8 +48,8 @@
     return jnp.where(y < 0.5, y * series, 1.0 - decay * decay)
 
 
-def kernel(n, tq, tok, gain, wxg, wo, maps, small, pj, out,
-           WX, WO, MAPS, SMALL, XM, XH, NRM, XR, GEL, BD, PAR, AS, BS, LOC, ACU, MIX, MX,
+def kernel(n, tq, tok, gain, xw, gw, wo, taps, am, im, rate, og, pace, jumps, out,
+           WXG, MAPO, SMO, PJ, WX, WO, MAPS, SMALL, XM, XH, NRM, XR, GEL, BD, PAR, AS, BS, LOC, ACU, MIX, MX,
            PO, PR, ZO, ZR, FS, OB, send, recv):
     nt, nz, ns = n * n, n * n, 2 * n * n
     C = n * HEAD
@@ -85,35 +85,101 @@
         pltpu.make_async_copy(ref, ref, recv.at[slot]).wait()
 
     near = range(1, n)
-
-    def z1_x(l):
-        return [put(wxg.at[l], WX.at[l, p, a, b, c], (((a + d) % n) * n + b) * 2 + c, tp) for d in near]
-
-    i0, i1 = a + c * (b - a), b + c * (a - b)
-
-    def z1_o(l):
-        return [put(wo.at[l], WO.at[l, p, i0, i1, c], (((a + d) % n) * n + b) * 2 + c, tp) for d in near]
-
-    def z2_x(l):
-        ref = WX.at[l, p, :, b, c]
-        return [put(ref, ref, (a * n + (b + d) % n) * 2 + c, tp) for d in near]
-
-    def z2_o(l):
-        made = []
+    half = n * n // 4
+    across = 1 - c
+
+    barrier = pltpu.get_barrier_semaphore()
+
+    def greet(sp_to, tp_to):
+        pl.semaphore_signal(barrier, inc=1, device_id={"sp": sp_to, "tp": tp_to},
+                            device_id_type=pl.DeviceIdType.MESH)
+
+    def zat(d, core=None):
+        return ((z + d + nz) % nz) * 2 + (c if core is None else core)
+
+    zs = sorted({d % nz for d in (1, 2, -1, -2)})
+    for d in near:
+        greet(s, tp_of(c, (p + d) % n, q))
+        greet(s, tp_of(c, p, (q + d) % n))
+    for d in range(n):
+        greet(z * 2 + across, tp_of(across, q, d))
+    for d in zs:
+        greet(zat(d), tp)
+
+    @pl.when((1 - c) * (1 - jnp.minimum(p, 1)) == 1)
+    def _():
+        for k in range(n):
+            greet(zat(-1, 1), tp_of(1, q, k))
+
+    for l in range(LAYERS):
+        WXG[l] = jnp.concatenate([xw[l], gw[l]], axis=1)
+        MAPO[l] = jnp.concatenate([am[l, 0], im[l, 0]], axis=1)
+        rows = jnp.concatenate(
+            [taps[l].astype(f32), rate[l:l + 1], og[l:l + 1].astype(f32), jnp.ones((2, HEAD), f32)], axis=0)
+        SMO[l] = jnp.concatenate([rows, rows], axis=1)
+    for i, ref in enumerate((pace, jumps)):
+        for r in range(n * tq // LANE):
+            PJ[i, r * LANE:(r + 1) * LANE] = jnp.transpose(jnp.broadcast_to(ref[r:r + 1], (LANE, LANE)))
+    pl.semaphore_wait(barrier, 2 * (n - 1) + n + len(zs) + c)
+
+    def x_piece(l, o):
+        return WX.at[l, p, o, c]
+
+    def o_piece(l, o):
+        i, k = o // n, o % n
+        return WO.at[l, p, i + c * (k - i), k + c * (i - k), c]
+
+    def ring_numbers():
+        first = next(numbers)
+        for _ in range(4 * half - 1):
+            next(numbers)
+        return first
+
+    def ring_send(piece, own, l, k, first):
+        for sign, i in ((1, 0), (-1, 2)):
+            o = (z - sign * 2 * k + nz) % nz
+            dst = piece(l, o)
+            src = own if k == 0 else dst
+            put(src, dst, zat(sign), tp, first + 4 * k + i)
+            if sign == 1 or k < half - 1:
+                put(src, dst, zat(2 * sign), tp, first + 4 * k + i + 1)
+
+    def ring_land(piece, l, k, first):
+        got = []
+        for sign, i in ((1, 0), (-1, 2)):
+            for j in (1, 2):
+                if j == 2 and sign == -1 and k == half - 1:
+                    continue
+                o = (z - sign * (2 * k + j) + nz) % nz
+                landed_all(piece(l, o), first + 4 * k + i + j - 1)
+                got.append(o)
+        return got
+
+    same, other = next(numbers), next(numbers)
+
+    def spread(o, src=None):
+        ref = WX.at[0, p, o, c]
+        src = ref if src is None else src
         for d in near:
+            put(src, ref, s, tp_of(c, (p + d) % n, q), same)
+        for d in range(n):
+            put(src, WX.at[0, q, o, c], z * 2 + across, tp_of(across, (q + d) % n, p), other)
+
+    def spread_x(l):
+        made = [put(WX.at[l, p, :, c], WX.at[l, p, :, c], s, tp_of(c, (p + d) % n, q)) for d in near]
+        for d in range(n):
+            made.append(put(WX.at[l, p, :, c], WX.at[l, q, :, c], z * 2 + across, tp_of(across, (q + d) % n, p)))
+        return made
+
+    def spread_o(l):
+        made = [put(WO.at[l, p, :, :, c], WO.at[l, p, :, :, c], s, tp_of(c, (p + d) % n, q)) for d in near]
+        for d in range(n):
             for k in range(n):
-                ref = WO.at[l, p, k + c * (b - k), b + c * (k - b), c]
-                made.append(put(ref, ref, (a * n + (b + d) % n) * 2 + c, tp))
+                made.append(put(WO.at[l, p, k, :, c], WO.at[l, q, :, k, c], z * 2 + across,
+                                tp_of(across, (q + d) % n, p)))
         return made
 
-    def twin_x(l):
-        return [put(WX.at[l, p, :, :, c], WX.at[l, q, :, :, c], z * 2 + 1 - c, tp)]
-
-    def twin_o(l):
-        return [put(WO.at[l, p, k, :, c], WO.at[l, q, :, k, c], z * 2 + 1 - c, tp) for k in range(n)]
-
-    def across(ref):
-        return [put(ref, ref, s, tp_of(c, (p + d) % n, q)) for d in near]
+    firsts = {(kind, l): ring_numbers() for l in range(LAYERS) for kind in "xo"}
 
     own = pl.ds(pl.multiple_of(p * tq, tq), tq)
     t_a = []
@@ -123,42 +189,44 @@
         t_a.append(put(tok.at[rows], XM.at[0, tp], s, tp_of(c, pp, q)))
     rim0 = next(numbers)
     rim_sends = []
-    for k in range(n):
-        e, pp = (k + 1) // n, (k + 1) % n
+    for k in range(n - 1):
         src = tok.at[(k + 1) * tq - RIM:(k + 1) * tq]
-        for qq in range(n):
-            cp = pltpu.make_async_remote_copy(
-                src_ref=src, dst_ref=XH.at[0, tp], send_sem=send, recv_sem=recv.at[rim0],
-                device_id={"sp": (s + e) % ns, "tp": tp_of((c + e) % 2, pp, qq)},
-                device_id_type=pl.DeviceIdType.MESH)
-            if e:
-                cp.start()
-                sent.append(cp)
-            else:
-                mine = (1 - jnp.minimum(abs(pp - p), 1)) * (1 - jnp.minimum(abs(qq - q), 1))
-
-                @pl.when(mine == 0)
-                def _():
-                    cp.start()
-
-                @pl.when(mine == 1)
-                def _():
-                    XH[0, tp] = src[...]
-                rim_sends.append((cp, mine))
-    wx = [z1_x(0), None]
-    wout = [z1_o(0), None]
-    m_in = [put(maps, MAPS.at[p], s, tp_of(c, (p + d) % n, q)) for d in near]
-    s_in = [put(small, SMALL.at[tp], s, (tp + d) % nt) for d in range(1, nt)]
-    wx[1], wout[1] = z1_x(1), z1_o(1)
+        cp = pltpu.make_async_remote_copy(
+            src_ref=src, dst_ref=XH.at[0, tp], send_sem=send, recv_sem=recv.at[rim0],
+            device_id={"sp": s, "tp": tp_of(c, k + 1, q)}, device_id_type=pl.DeviceIdType.MESH)
+
+        @pl.when(p != k + 1)
+        def _():
+            cp.start()
+
+        @pl.when(p == k + 1)
+        def _():
+            XH[0, tp] = src[...]
+        rim_sends.append((cp, k + 1))
+    put(tok.at[n * tq - RIM:n * tq], XH.at[0, tp], (s + 1) % ns, tp_of(across, 0, p), rim0)
+    ring_send(x_piece, WXG.at[0], 0, 0, firsts["x", 0])
+    spread(z, WXG.at[0])
+    m_in = [put(MAPO, MAPS.at[p], s, tp_of(c, (p + d) % n, q)) for d in near]
+    s_in = [put(SMO, SMALL.at[p], s, tp_of(c, (p + d) % n, q)) for d in near]
+    ring_send(o_piece, wo.at[0], 0, 0, firsts["o", 0])
 
     XM[0, tp] = tok[own]
     for l in range(LAYERS):
-        WX[l, p, a, b, c] = wxg[l]
-        WO[l, p, i0, i1, c] = wo[l]
-    MAPS[p] = maps[...]
-    SMALL[tp] = small[...]
+        WX[l, p, z, c] = WXG[l]
+        WO[l, p, a + c * (b - a), b + c * (a - b), c] = wo[l]
+    MAPS[p] = MAPO[...]
+    SMALL[p] = SMO[...]
 
     landed(t_a)
+
+    @pl.when(p > 0)
+    def _():
+        landed_all(XH.at[0, :n - 1], rim0)
+
+    @pl.when(p == 0)
+    def _():
+        landed_all(XH.at[0, :n], rim0)
+
     t_b = []
     for d in near:
         to = tp_of(c, p, (q + d) % n)
@@ -166,11 +234,32 @@
         for e in near:
             ref = XM.at[0, tp_of(c, (p + e) % n, q)]
             t_b.append(put(ref, ref, s, to))
-
-    landed(wx[0])
-    wx[0] = z2_x(0)
-    landed(wout[0])
-    wout[0] = z2_o(0)
+        for e in range(n):
+            ref = XH.at[0, tp_of(c, (p + e) % n, q)]
+            t_b.append(put(ref, ref, s, to))
+
+    def ring_step(k):
+        if k < half:
+            got = ring_land(x_piece, 0, k - 1, firsts["x", 0])
+            ring_send(x_piece, None, 0, k, firsts["x", 0])
+        else:
+            got = ring_land(x_piece, 0, half - 1, firsts["x", 0])
+        for o in got:
+            spread(o)
+        ring_land(o_piece, 0, k - 1, firsts["o", 0])
+        if k < half:
+            ring_send(o_piece, None, 0, k, firsts["o", 0])
+
+    def ring_step1(k):
+        for kind, piece, mine in (("x", x_piece, WXG), ("o", o_piece, wo)):
+            if k > 0:
+                ring_land(piece, 1, k - 1, firsts[kind, 1])
+            if k < half:
+                ring_send(piece, mine.at[1], 1, k, firsts[kind, 1])
+
+    for k in range(1, half):
+        ring_step(k)
+        ring_step1(k - 1)
 
     landed(m_in)
     landed(s_in)
@@ -183,8 +272,7 @@
             BD[l, jp, :HEAD, LANE:] = jnp.where(low, swapped(even), 0.0).astype(bf16)
             BD[l, jp, HEAD:, :LANE] = jnp.where(low, 0.0, swapped(odd)).astype(bf16)
             BD[l, jp, HEAD:, LANE:] = jnp.where(low, 0.0, odd).astype(bf16)
-            for qq in range(n):
-                PAR[l, qq, jp] = halves(SMALL[tp_of(c, 2 * jp, qq), l], SMALL[tp_of(c, 2 * jp + 1, qq), l])
+            PAR[l, q, jp] = halves(SMALL[2 * jp, l], SMALL[2 * jp + 1, l])
 
     def norm_rows(l, block, row):
         total = jnp.zeros((RIM, LANE), f32)
@@ -208,8 +296,8 @@
     def first_half(l):
         keep = jnp.minimum(s + p, 1).astype(f32)
         normed = NRM[...]
-        pace = pj[own, 0:1]
-        jump = pj[own, 1:2]
+        speed = PJ[0, own, :]
+        jump = PJ[1, own, :]
         for jp in range(pairs):
             w = jnp.concatenate(
                 [WX[l, 2 * jp].reshape(D, LANE), WX[l, 2 * jp + 1].reshape(D, LANE)], axis=1)
@@ -227,7 +315,7 @@
             gates = jnp.dot(xc, BD[l, jp], preferred_element_type=f32)
             r = jax.nn.sigmoid(gates[:, :LANE])
             gin = jax.nn.sigmoid(gates[:, LANE:])
-            log_a = -GATE_C * r * par[4:5] * pace + jump
+            log_a = -GATE_C * r * par[4:5] * speed + jump
             decay = jnp.exp(log_a)
             AS[jp] = decay
             BS[jp] = jnp.sqrt(one_minus_exp(-2.0 * log_a, decay)) * gin * xc.astype(f32)
@@ -311,42 +399,21 @@
                 at = tp_of(c, 2 * jp + j, q)
                 emit(2 * jp + j, (XM[l, at].astype(f32) + up[:, j * LANE:(j + 1) * LANE]).astype(bf16))
 
+    par_in = [put(PAR.at[:, q], PAR.at[:, q], s, tp_of(c, p, (q + d) % n)) for d in near]
     landed(t_b)
-
-    @pl.when(p > 0)
-    def _():
-        landed_all(XH.at[0, :nt - 1], rim0)
-
-    @pl.when(p == 0)
-    def _():
-        landed_all(XH.at[0], rim0)
-
+    ring_step(half)
+    ring_step1(half - 1)
+    o_in = [spread_o(0), None]
     norm(0)
-    landed(wx[0])
-    wx[0] = twin_x(0)
-    landed(wout[0])
-    wout[0] = twin_o(0)
-    landed(wx[0])
-    wx[0] = across(WX.at[0, p])
-    landed(wout[0])
-    wout[0] = across(WO.at[0, p])
-    landed(wx[1])
-    wx[1] = z2_x(1)
-    landed(wout[1])
-    wout[1] = z2_o(1)
-    landed(wx[0])
+    ring_step1(half)
+    x_in = spread_x(1)
+    landed_all(WX.at[0, 0:n - 1, :, 0], same)
+    landed_all(WX.at[0, :, :, 0], other)
     start = first_half(0)
-    landed(wx[1])
-    wx[1] = twin_x(1)
-    landed(wout[1])
-    wout[1] = twin_o(1)
     incoming = prefix(0)
     gathered = second_half(0, start, incoming)
-    landed(wx[1])
-    wx[1] = across(WX.at[1, p])
-    landed(wout[1])
-    wout[1] = across(WO.at[1, p])
-    landed(wout[0])
+    landed(par_in)
+    landed(o_in[0])
     landed(gathered)
 
     def keep_stream(j, v):
@@ -367,11 +434,12 @@
     landed(gathered)
     landed_all(XH.at[1], rim1)
     norm(1)
-    landed(wx[1])
+    landed(x_in)
     start = first_half(1)
+    o_in[1] = spread_o(1)
     incoming = prefix(1)
     gathered = second_half(1, start, incoming)
-    landed(wout[1])
+    landed(o_in[1])
     landed(gathered)
 
     def keep_last(j, v):
@@ -385,8 +453,8 @@
         out[k * tq:(k + 1) * tq] = OB[k]
     for cp in sent:
         cp.wait_send()
-    for cp, mine in rim_sends:
-        @pl.when(mine == 0)
+    for cp, k in rim_sends:
+        @pl.when(p != k)
         def _():
             cp.wait_send()
 
@@ -398,20 +466,18 @@
     tq = tokens.shape[0] // n
     C = n * HEAD
     D = nt * LANE
-    wxg = jnp.concatenate([x_weight, gate_weight], axis=2)
-    maps = jnp.concatenate([a_maps[:, 0], i_maps[:, 0]], axis=2)
-    small = jnp.concatenate(
-        [conv_taps.astype(f32), decay_rate[:, None], out_gain.astype(f32)[:, None],
-         jnp.ones((LAYERS, 2, HEAD), f32)], axis=1)
-    small = jnp.concatenate([small, small], axis=2)
-    pj = jnp.stack([pace, jumps], axis=1)
+    lines = (-1, LANE)
     vmem = pl.BlockSpec(memory_space=pltpu.VMEM)
-    xr, orr = wxg.shape[1], out_weight.shape[1]
+    xr, orr = x_weight.shape[1], out_weight.shape[1]
     scratch = [
-        pltpu.VMEM((LAYERS, n, n, n, 2, xr, LANE), bf16),
+        pltpu.VMEM((LAYERS, xr, LANE), bf16),
+        pltpu.VMEM((LAYERS, HEAD, LANE), bf16),
+        pltpu.VMEM((LAYERS, ROWS, LANE), f32),
+        pltpu.VMEM((2, n * tq, LANE), f32),
+        pltpu.VMEM((LAYERS, n, nt, 2, xr, LANE), bf16),
         pltpu.VMEM((LAYERS, n, n, n, 2, orr, LANE), bf16),
         pltpu.VMEM((n, LAYERS, HEAD, LANE), bf16),
-        pltpu.VMEM((nt, LAYERS, ROWS, LANE), f32),
+        pltpu.VMEM((n, LAYERS, ROWS, LANE), f32),
         pltpu.VMEM((LAYERS, nt, tq, LANE), bf16),
         pltpu.VMEM((LAYERS, nt, RIM, LANE), bf16),
         pltpu.VMEM((RIM + tq, D), bf16),
@@ -432,16 +498,17 @@
         pltpu.VMEM((n, tq, LANE), bf16),
         pltpu.VMEM((n, tq, LANE), bf16),
         pltpu.SemaphoreType.DMA,
-        pltpu.SemaphoreType.DMA((256,)),
+        pltpu.SemaphoreType.DMA((320,)),
     ]
     return pl.pallas_call(
         functools.partial(kernel, n, tq),
         out_shape=jax.ShapeDtypeStruct(tokens.shape, bf16),
-        in_specs=[vmem] * 7,
+        in_specs=[vmem] * 12,
         out_specs=vmem,
         scratch_shapes=scratch,
-        compiler_params=pltpu.CompilerParams(has_side_effects=True, vmem_limit_bytes=56 * 1024 * 1024),
-    )(tokens, mix_gain, wxg, out_weight, maps, small, pj)
+        compiler_params=pltpu.CompilerParams(collective_id=0, has_side_effects=True, vmem_limit_bytes=56 * 1024 * 1024),
+    )(tokens, mix_gain, x_weight, gate_weight, out_weight, conv_taps, a_maps, i_maps, decay_rate, out_gain,
+      pace.reshape(lines), jumps.reshape(lines))
 
 
 def solution(mesh):

time: 141 us -> 108 us (0.77)
  Pallas kernels: 133 us -> 106 us
  local copies, waits for them, and re-layouts: 5.29 us -> 1.62 us
  other arithmetic: 2.85 us -> 0 us
    pallas_call x1, Pallas kernels: 133 us -> 106 us  [body(): pl.pallas_call(functools.partial(kernel, n, tq), out_shape=jax.ShapeDtype...]
    another operation x3 -> x0, local copies, waits for them, and re-layouts: 2.32 us -> none  [body(): pj = jnp.stack([pace, jumps], axis=1)]
    concatenate x2 -> x0, other arithmetic: 2.17 us -> none  [the longest x1 1.5 us: body(): wxg = jnp.concatenate([x_weight, gate_weight], axis=2)]
    unnamed x7 -> x1, local copies, waits for them, and re-layouts: 2.97 us -> 1.62 us
where the time goes in v2:
time: 108 us
  Pallas kernels  106 us (98%)
  local copies, waits for them, and re-layouts  1.62 us (2%)
    pallas_call x1, Pallas kernels, body(): pl.pallas_call(functools.partial(kernel, n, tq), out_shape=jax.ShapeDtype...  106 us

profile of v2, /device:TPU:1, one launch (start us, length us, event | category | flops | bytes accessed | tf_op | source)
XLA Modules:
  0.0 108.1 jit_solution(8426700046608900440)
XLA Ops:
  0.0 106.4 %shard_map.118 = bf16[768,128]{1,0:T(8,128)(2,1)} custom-call(bf16[768,128]{1,0:T(8,128)(2,1)} %tok.1, bf16[2,2048]{1,0:T(2,128)(2,1)} %gain.1, bf16[2,64,64]{2,1,0:T(8,128)(2,1)} %xw.1, bf16[2,64,64]{2,1,0:T(8,128)(2,1)} %gw.1, bf16[2,32,128]{2,1,0:T(8,128)(2,1)} %wo.1, bf16[2,4,64]{2,1,0:T(4,128)(2,1)} %taps.1, bf16[2,1,64,64]{3,2,1,0:T(8,128)(2,1)} %am.1, ...), custom_call_target="tpu_custom_call" | custom-call | tf_op jit(solution)/shard_map/pallas_call | solution.py:503
  106.4 1.6 %copy.14 = bf16[768,128]{1,0:T(8,128)(2,1)} copy(bf16[768,128]{1,0:T(8,128)(2,1)} %shard_map.118) | data formatting | bytes 393216

commit v3 on v2

--- a/solution.py
+++ b/solution.py
@@ -165,10 +165,29 @@
         for d in range(n):
             put(src, WX.at[0, q, o, c], z * 2 + across, tp_of(across, (q + d) % n, p), other)
 
-    def spread_x(l):
-        made = [put(WX.at[l, p, :, c], WX.at[l, p, :, c], s, tp_of(c, (p + d) % n, q)) for d in near]
+    def spread_x(l, first, last):
+        part = pl.ds(first, last - first)
+        made = [put(WX.at[l, p, part, c], WX.at[l, p, part, c], s, tp_of(c, (p + d) % n, q)) for d in near]
         for d in range(n):
-            made.append(put(WX.at[l, p, :, c], WX.at[l, q, :, c], z * 2 + across, tp_of(across, (q + d) % n, p)))
+            made.append(put(WX.at[l, p, part, c], WX.at[l, q, part, c], z * 2 + across,
+                            tp_of(across, (q + d) % n, p)))
+        return made
+
+    def far_first(l):
+        made = []
+        for d in near:
+            to = (((a + d) % n) * n + b) * 2 + c
+            made.append(put(WXG.at[l], x_piece(l, z), to, tp))
+            made.append(put(wo.at[l], o_piece(l, z), to, tp))
+        return made
+
+    def near_next(l):
+        made = []
+        for piece in (x_piece, o_piece):
+            for d in near:
+                for k in range(n):
+                    ref = piece(l, k * n + b)
+                    made.append(put(ref, ref, (a * n + (b + d) % n) * 2 + c, tp))
         return made
 
     def spread_o(l):
@@ -179,7 +198,7 @@
                                 tp_of(across, (q + d) % n, p)))
         return made
 
-    firsts = {(kind, l): ring_numbers() for l in range(LAYERS) for kind in "xo"}
+    firsts = {(kind, 0): ring_numbers() for kind in "xo"}
 
     own = pl.ds(pl.multiple_of(p * tq, tq), tq)
     t_a = []
@@ -250,16 +269,8 @@
         if k < half:
             ring_send(o_piece, None, 0, k, firsts["o", 0])
 
-    def ring_step1(k):
-        for kind, piece, mine in (("x", x_piece, WXG), ("o", o_piece, wo)):
-            if k > 0:
-                ring_land(piece, 1, k - 1, firsts[kind, 1])
-            if k < half:
-                ring_send(piece, mine.at[1], 1, k, firsts[kind, 1])
-
     for k in range(1, half):
         ring_step(k)
-        ring_step1(k - 1)
 
     landed(m_in)
     landed(s_in)
@@ -340,7 +351,7 @@
                            jnp.where(row >= 1, pltpu.roll(h, 1, 0), 0.0)))
         return starts
 
-    def prefix(l):
+    def prefix(l, meanwhile):
         made = []
         for d in near:
             made.append(put(PO.at[l], PR.at[l, c, p], s, tp_of(c, (p + d) % n, q)))
@@ -364,6 +375,7 @@
         slot = next(numbers)
         for d in range(1, nz):
             put(ZO.at[l], ZR.at[l, d - 1], ((z + d) % nz) * 2 + c, tp, slot)
+        meanwhile()
         landed_all(ZR.at[l], slot)
         before = identity
         for d in range(nz - 1, 0, -1):
@@ -401,17 +413,30 @@
 
     par_in = [put(PAR.at[:, q], PAR.at[:, q], s, tp_of(c, p, (q + d) % n)) for d in near]
     landed(t_b)
+    l1_in = [far_first(1) if half > 1 else []]
     ring_step(half)
-    ring_step1(half - 1)
+    if half == 1:
+        l1_in = [far_first(1)]
     o_in = [spread_o(0), None]
     norm(0)
-    ring_step1(half)
-    x_in = spread_x(1)
     landed_all(WX.at[0, 0:n - 1, :, 0], same)
     landed_all(WX.at[0, :, :, 0], other)
+    landed(l1_in[0])
+    l1_in.append(near_next(1))
     start = first_half(0)
-    incoming = prefix(0)
+    x_in = []
+    cut = 3 * nt // 4
+
+    def send_x():
+        landed(l1_in[1])
+        x_in.extend(spread_x(1, 0, cut))
+
+    def send_o():
+        o_in[1] = spread_o(1)
+
+    incoming = prefix(0, send_x)
     gathered = second_half(0, start, incoming)
+    x_in.extend(spread_x(1, cut, nt))
     landed(par_in)
     landed(o_in[0])
     landed(gathered)
@@ -436,8 +461,7 @@
     norm(1)
     landed(x_in)
     start = first_half(1)
-    o_in[1] = spread_o(1)
-    incoming = prefix(1)
+    incoming = prefix(1, send_o)
     gathered = second_half(1, start, incoming)
     landed(o_in[1])
     landed(gathered)

time: 108 us -> 102 us (0.944)
  Pallas kernels: 106 us -> 100 us
    pallas_call x1, Pallas kernels: 106 us -> 100 us  [body(): pl.pallas_call(functools.partial(kernel, n, tq), out_shape=jax.ShapeDtype...]
where the time goes in v3:
time: 102 us
  Pallas kernels  100 us (98%)
  local copies, waits for them, and re-layouts  1.62 us (2%)
    pallas_call x1, Pallas kernels, body(): pl.pallas_call(functools.partial(kernel, n, tq), out_shape=jax.ShapeDtype...  100 us

profile of v3, /device:TPU:1, one launch (start us, length us, event | category | flops | bytes accessed | tf_op | source)
XLA Modules:
  0.0 101.9 jit_solution(17640678585278658129)
XLA Ops:
  0.0 100.3 %shard_map.118 = bf16[768,128]{1,0:T(8,128)(2,1)} custom-call(bf16[768,128]{1,0:T(8,128)(2,1)} %tok.1, bf16[2,2048]{1,0:T(2,128)(2,1)} %gain.1, bf16[2,64,64]{2,1,0:T(8,128)(2,1)} %xw.1, bf16[2,64,64]{2,1,0:T(8,128)(2,1)} %gw.1, bf16[2,32,128]{2,1,0:T(8,128)(2,1)} %wo.1, bf16[2,4,64]{2,1,0:T(4,128)(2,1)} %taps.1, bf16[2,1,64,64]{3,2,1,0:T(8,128)(2,1)} %am.1, ...), custom_call_target="tpu_custom_call" | custom-call | tf_op jit(solution)/shard_map/pallas_call | solution.py:527
  100.3 1.6 %copy.14 = bf16[768,128]{1,0:T(8,128)(2,1)} copy(bf16[768,128]{1,0:T(8,128)(2,1)} %shard_map.118) | data formatting | bytes 393216

commit v4 on v3

--- a/solution.py
+++ b/solution.py
@@ -85,7 +85,8 @@
         pltpu.make_async_copy(ref, ref, recv.at[slot]).wait()
 
     near = range(1, n)
-    half = n * n // 4
+    reach = min(4, nz // 2)
+    half = nz // 2 // reach
     across = 1 - c
 
     barrier = pltpu.get_barrier_semaphore()
@@ -97,7 +98,7 @@
     def zat(d, core=None):
         return ((z + d + nz) % nz) * 2 + (c if core is None else core)
 
-    zs = sorted({d % nz for d in (1, 2, -1, -2)})
+    zs = sorted({d % nz for d in range(-reach, reach + 1)} - {0})
     for d in near:
         greet(s, tp_of(c, (p + d) % n, q))
         greet(s, tp_of(c, p, (q + d) % n))
@@ -129,30 +130,26 @@
         i, k = o // n, o % n
         return WO.at[l, p, i + c * (k - i), k + c * (i - k), c]
 
+    def hops(k):
+        for sign, i in ((1, 0), (-1, reach)):
+            for j in range(1, reach + 1):
+                if sign == 1 or j < reach or k < half - 1:
+                    yield sign, j, 2 * reach * k + i + j - 1
+
     def ring_numbers():
-        first = next(numbers)
-        for _ in range(4 * half - 1):
-            next(numbers)
-        return first
-
-    def ring_send(piece, own, l, k, first):
-        for sign, i in ((1, 0), (-1, 2)):
-            o = (z - sign * 2 * k + nz) % nz
-            dst = piece(l, o)
-            src = own if k == 0 else dst
-            put(src, dst, zat(sign), tp, first + 4 * k + i)
-            if sign == 1 or k < half - 1:
-                put(src, dst, zat(2 * sign), tp, first + 4 * k + i + 1)
-
-    def ring_land(piece, l, k, first):
+        return [next(numbers) for _ in range(2 * reach * half)]
+
+    def ring_send(piece, own, l, k, slots):
+        for sign, j, i in hops(k):
+            dst = piece(l, (z - sign * reach * k + nz) % nz)
+            put(own if k == 0 else dst, dst, zat(sign * j), tp, slots[i])
+
+    def ring_land(piece, l, k, slots):
         got = []
-        for sign, i in ((1, 0), (-1, 2)):
-            for j in (1, 2):
-                if j == 2 and sign == -1 and k == half - 1:
-                    continue
-                o = (z - sign * (2 * k + j) + nz) % nz
-                landed_all(piece(l, o), first + 4 * k + i + j - 1)
-                got.append(o)
+        for sign, j, i in hops(k):
+            o = (z - sign * (reach * k + j) + nz) % nz
+            landed_all(piece(l, o), slots[i])
+            got.append(o)
         return got
 
     same, other = next(numbers), next(numbers)
@@ -412,17 +409,15 @@
                 emit(2 * jp + j, (XM[l, at].astype(f32) + up[:, j * LANE:(j + 1) * LANE]).astype(bf16))
 
     par_in = [put(PAR.at[:, q], PAR.at[:, q], s, tp_of(c, p, (q + d) % n)) for d in near]
+    l1_in = [far_first(1)]
     landed(t_b)
-    l1_in = [far_first(1) if half > 1 else []]
     ring_step(half)
-    if half == 1:
-        l1_in = [far_first(1)]
     o_in = [spread_o(0), None]
     norm(0)
+    landed(l1_in[0])
+    l1_in.append(near_next(1))
     landed_all(WX.at[0, 0:n - 1, :, 0], same)
     landed_all(WX.at[0, :, :, 0], other)
-    landed(l1_in[0])
-    l1_in.append(near_next(1))
     start = first_half(0)
     x_in = []
     cut = 3 * nt // 4
@@ -436,7 +431,6 @@
 
     incoming = prefix(0, send_x)
     gathered = second_half(0, start, incoming)
-    x_in.extend(spread_x(1, cut, nt))
     landed(par_in)
     landed(o_in[0])
     landed(gathered)
@@ -456,6 +450,7 @@
         at = tp_of(c, j, q)
         for qq in range(n):
             put(XM.at[1, at, tq - RIM:tq], XH.at[1, at], (s + e) % ns, tp_of((c + e) % 2, pp, qq), rim1)
+    x_in.extend(spread_x(1, cut, nt))
     landed(gathered)
     landed_all(XH.at[1], rim1)
     norm(1)

time: 102 us -> 97.8 us (0.959)
  Pallas kernels: 100 us -> 95.7 us
    pallas_call x1, Pallas kernels: 100 us -> 95.7 us  [body(): pl.pallas_call(functools.partial(kernel, n, tq), out_shape=jax.ShapeDtype...]
where the time goes in v4:
time: 97.8 us; the launch traced here: 97.3 us
  Pallas kernels  95.7 us (98%)
  local copies, waits for them, and re-layouts  1.62 us (2%)
    pallas_call x1, Pallas kernels, body(): pl.pallas_call(functools.partial(kernel, n, tq), out_shape=jax.ShapeDtype...  95.7 us

profile of v4, /device:TPU:1, one launch (start us, length us, event | category | flops | bytes accessed | tf_op | source)
XLA Modules:
  0.0 97.3 jit_solution(13391280723163361465)
XLA Ops:
  0.0 95.7 %shard_map.118 = bf16[768,128]{1,0:T(8,128)(2,1)} custom-call(bf16[768,128]{1,0:T(8,128)(2,1)} %tok.1, bf16[2,2048]{1,0:T(2,128)(2,1)} %gain.1, bf16[2,64,64]{2,1,0:T(8,128)(2,1)} %xw.1, bf16[2,64,64]{2,1,0:T(8,128)(2,1)} %gw.1, bf16[2,32,128]{2,1,0:T(8,128)(2,1)} %wo.1, bf16[2,4,64]{2,1,0:T(4,128)(2,1)} %taps.1, bf16[2,1,64,64]{3,2,1,0:T(8,128)(2,1)} %am.1, ...), custom_call_target="tpu_custom_call" | custom-call | tf_op jit(solution)/shard_map/pallas_call | solution.py:522
  95.7 1.6 %copy.14 = bf16[768,128]{1,0:T(8,128)(2,1)} copy(bf16[768,128]{1,0:T(8,128)(2,1)} %shard_map.118) | data formatting | bytes 393216

commit v5 on v4

--- a/solution.py
+++ b/solution.py
@@ -234,15 +234,6 @@
     SMALL[p] = SMO[...]
 
     landed(t_a)
-
-    @pl.when(p > 0)
-    def _():
-        landed_all(XH.at[0, :n - 1], rim0)
-
-    @pl.when(p == 0)
-    def _():
-        landed_all(XH.at[0, :n], rim0)
-
     t_b = []
     for d in near:
         to = tp_of(c, p, (q + d) % n)
@@ -250,9 +241,19 @@
         for e in near:
             ref = XM.at[0, tp_of(c, (p + e) % n, q)]
             t_b.append(put(ref, ref, s, to))
+
+    @pl.when(p > 0)
+    def _():
+        landed_all(XH.at[0, :n - 1], rim0)
+
+    @pl.when(p == 0)
+    def _():
+        landed_all(XH.at[0, :n], rim0)
+
+    for d in near:
         for e in range(n):
             ref = XH.at[0, tp_of(c, (p + e) % n, q)]
-            t_b.append(put(ref, ref, s, to))
+            t_b.append(put(ref, ref, s, tp_of(c, p, (q + d) % n)))
 
     def ring_step(k):
         if k < half:

time: 97.8 us -> 97.7 us (level)
  no operation moved by 1% of the time
where the time goes in v5:
time: 97.7 us; the launch traced here: 97.2 us
  Pallas kernels  95.6 us (98%)
  local copies, waits for them, and re-layouts  1.62 us (2%)
    pallas_call x1, Pallas kernels, body(): pl.pallas_call(functools.partial(kernel, n, tq), out_shape=jax.ShapeDtype...  95.6 us

profile of v5, /device:TPU:1, one launch (start us, length us, event | category | flops | bytes accessed | tf_op | source)
XLA Modules:
  0.0 97.2 jit_solution(907097853540754507)
XLA Ops:
  0.0 95.6 %shard_map.118 = bf16[768,128]{1,0:T(8,128)(2,1)} custom-call(bf16[768,128]{1,0:T(8,128)(2,1)} %tok.1, bf16[2,2048]{1,0:T(2,128)(2,1)} %gain.1, bf16[2,64,64]{2,1,0:T(8,128)(2,1)} %xw.1, bf16[2,64,64]{2,1,0:T(8,128)(2,1)} %gw.1, bf16[2,32,128]{2,1,0:T(8,128)(2,1)} %wo.1, bf16[2,4,64]{2,1,0:T(4,128)(2,1)} %taps.1, bf16[2,1,64,64]{3,2,1,0:T(8,128)(2,1)} %am.1, ...), custom_call_target="tpu_custom_call" | custom-call | tf_op jit(solution)/shard_map/pallas_call | solution.py:523
  95.6 1.6 %copy.14 = bf16[768,128]{1,0:T(8,128)(2,1)} copy(bf16[768,128]{1,0:T(8,128)(2,1)} %shard_map.118) | data formatting | bytes 393216
